TPU v7x, 32 devices: a whole 2x2x4 slice. The times are simulated.
32 devices in a mesh: rep: 2 (over x), fs: 8 (over z, y), tp: 2 (over core).
Axes of the slice: x: 2, y: 2, z: 4, core: 2. Of those that a mesh axis runs over, the one named last changes fastest.
Arguments:
- tokens: bfloat16 [16384, 2048], P(('rep', 'fs')), may hold values from -6 to 6
- norm_mix: bfloat16 [2048], replicated, may hold values from 0.099609375 to 1.8984375
- w_unit: bfloat16 [2048, 1024], P('fs', 'tp'), may hold values from -0.125 to 0.125
- w_value: bfloat16 [2048, 1024], P('fs', 'tp'), may hold values from -0.125 to 0.125
- spatial: bfloat16 [4, 128, 128], replicated, may hold values from -0.52734375 to 0.52734375
- spatial_bias: bfloat16 [4, 128], replicated, may hold values from 0.099609375 to 1.8984375
- group_gain: bfloat16 [1024], replicated, may hold values from 0.099609375 to 1.8984375
- group_shift: bfloat16 [1024], replicated, may hold values from -3 to 3
- w_mix_out: bfloat16 [1024, 2048], P('tp', 'fs'), may hold values from -0.1875 to 0.1875
- norm_ffn: bfloat16 [2048], replicated, may hold values from 0.099609375 to 1.8984375
- w_gate: bfloat16 [2048, 2816], P('fs', 'tp'), may hold values from -0.125 to 0.125
- w_up: bfloat16 [2048, 2816], P('fs', 'tp'), may hold values from -0.125 to 0.125
- w_down: bfloat16 [2816, 2048], P('tp', 'fs'), may hold values from -0.109375 to 0.109375
Outputs:
- layer_out: bfloat16 [16384, 2048], P(('rep', 'fs', 'tp'))
All inputs are finite; a program needn't handle non-finite values.
Results may differ from a plain program's by a relative error of at most 0.008.
Values may be sent and summed in bfloat16 or wider, within the bound.
A program may use at most 128 MiB of HBM per device.

v0:
```python
import jax
import jax.numpy as jnp
from jax import lax
from jax.sharding import PartitionSpec as P


def rms_scale(values, gain):
    values = values.astype(jnp.float32)
    scale = lax.rsqrt(jnp.mean(values * values, axis=-1, keepdims=True) + 1e-06)
    return values * scale * gain.astype(jnp.float32)


def spatial_unit(unit_pre, value_pre, spatial, spatial_bias, group_gain, group_shift):
    count, width = value_pre.shape
    groups = spatial.shape[0]
    block = spatial.shape[1]
    active = jax.nn.gelu(value_pre, approximate=True).reshape(count, groups, width // groups)
    center = jnp.mean(active, axis=-1, keepdims=True)
    spread = jnp.mean(jnp.square(active - center), axis=-1, keepdims=True)
    normal = ((active - center) * lax.rsqrt(spread + 1e-06)).reshape(count, width)
    normal = normal * group_gain.astype(jnp.float32) + group_shift.astype(jnp.float32)
    grouped = normal.astype(jnp.bfloat16)
    causal = jnp.tril(jnp.ones((block, block), dtype=bool))
    weights = jnp.where(causal[None], spatial, jnp.zeros_like(spatial))
    tiles = grouped.reshape(count // block, block, groups, width // groups)
    mixed = jnp.einsum("gts,nsgd->ntgd", weights, tiles, preferred_element_type=jnp.float32)
    mixed = mixed + spatial_bias.astype(jnp.float32).T[None, :, :, None]
    return jax.nn.gelu(unit_pre, approximate=True) * mixed.reshape(count, width)


def on_device(
    tokens,
    norm_mix,
    w_unit,
    w_value,
    spatial,
    spatial_bias,
    group_gain,
    group_shift,
    w_mix_out,
    norm_ffn,
    w_gate,
    w_up,
    w_down,
):
    count = tokens.shape[0]
    half = count // lax.axis_size("tp")
    position = lax.axis_index("tp")
    row_start = position * half
    local_width = w_unit.shape[1]
    group_count = spatial.shape[0] // lax.axis_size("tp")
    group_start = position * group_count
    spatial_local = lax.dynamic_slice_in_dim(spatial, group_start, group_count, 0)
    bias_local = lax.dynamic_slice_in_dim(spatial_bias, group_start, group_count, 0)
    gain_local = lax.dynamic_slice_in_dim(group_gain, position * local_width, local_width, 0)
    shift_local = lax.dynamic_slice_in_dim(group_shift, position * local_width, local_width, 0)
    normed = rms_scale(tokens, norm_mix).astype(jnp.bfloat16)
    unit_whole, value_whole = (
        lax.all_gather(w_unit, "fs", axis=0, tiled=True),
        lax.all_gather(w_value, "fs", axis=0, tiled=True),
    )
    unit_pre = jnp.dot(normed, unit_whole, preferred_element_type=jnp.float32)
    value_pre = jnp.dot(normed, value_whole, preferred_element_type=jnp.float32)
    gated = spatial_unit(
        unit_pre, value_pre, spatial_local, bias_local, gain_local, shift_local
    ).astype(jnp.bfloat16)
    token_rows = lax.all_to_all(gated, "tp", split_axis=0, concat_axis=1, tiled=True)
    out_columns = lax.all_gather(w_mix_out, "fs", axis=1, tiled=True)
    out_whole = lax.all_gather(out_columns, "tp", axis=0, tiled=True)
    own_rows = lax.dynamic_slice_in_dim(tokens, row_start, half, 0)
    own_mid = (
        own_rows.astype(jnp.float32)
        + jnp.dot(token_rows, out_whole, preferred_element_type=jnp.float32)
    ).astype(jnp.bfloat16)
    h_mid = lax.all_gather(own_mid, "tp", axis=0, tiled=True)
    normed_mid = rms_scale(h_mid, norm_ffn).astype(jnp.bfloat16)
    gate_whole, up_whole = (
        lax.all_gather(w_gate, "fs", axis=0, tiled=True),
        lax.all_gather(w_up, "fs", axis=0, tiled=True),
    )
    gate = jnp.dot(normed_mid, gate_whole, preferred_element_type=jnp.float32)
    up = jnp.dot(normed_mid, up_whole, preferred_element_type=jnp.float32)
    hidden = (jax.nn.silu(gate) * up).astype(jnp.bfloat16)
    down_cols = lax.all_gather(w_down, "fs", axis=1, tiled=True)
    residual_rows = lax.dynamic_slice_in_dim(h_mid, row_start, half, 0).astype(jnp.float32)
    hidden_rows = lax.all_to_all(hidden, "tp", split_axis=0, concat_axis=1, tiled=True)
    down_full = lax.all_gather(down_cols, "tp", axis=0, tiled=True)
    summed_rows = jnp.dot(hidden_rows, down_full, preferred_element_type=jnp.float32)
    return (residual_rows + summed_rows).astype(jnp.bfloat16)


def solution(mesh):
    placed = (
        P(("rep", "fs"), None),
        P(),
        P("fs", "tp"),
        P("fs", "tp"),
        P(),
        P(),
        P(),
        P(),
        P("tp", "fs"),
        P(),
        P("fs", "tp"),
        P("fs", "tp"),
        P("tp", "fs"),
    )
    return jax.shard_map(
        on_device,
        mesh=mesh,
        in_specs=placed,
        out_specs=P(("rep", "fs", "tp"), None),
        check_vma=False,
    )
```

profile of v0, /device:TPU:0, one launch (start us, length us, event | category | flops | bytes accessed | tf_op | source)
XLA Modules:
  0.0 516.4 jit_solution(7229913326769791295)
XLA Ops:
  6.5 0.0 all-gather.14.cloned.1.call-start
  6.5 0.7 all-gather.14.cloned.1.call-update
  7.3 0.0 all-gather.12.cloned.1.call-start
  7.3 0.7 all-gather.12.cloned.1.call-update
  8.0 0.0 all-gather.10.cloned.1.call-start
  8.1 0.7 all-gather.10.cloned.1.call-update
  8.7 0.0 all-gather.16.cloned.1.call-start
  8.8 53.7 %all-gather.14.cloned.1.call-done = bf16[512,2048]{1,0:T(8,128)(2,1)} async-done(((bf16[512,256]{1,0:T(8,128)(2,1)}), bf16[512,2048]{1,0:T(8,128)(2,1)}) %all-gather.14.cloned.1.call-update) | async-done | bytes 2097168 | tf_op jit(solution)/shard_map/all_gather | solution.py:68
  62.5 0.0 all-gather.16.cloned.1.call-update
  62.5 0.0 all-gather.24.cloned.1.call-start
  62.5 0.5 all-gather.24.cloned.1.call-update
  63.1 0.0 all-gather.18.cloned.1.call-start
  63.1 0.7 convert_element_type.48
  63.8 0.7 convert_bitcast_fusion
  64.5 0.8 dynamic-slice_convert_fusion
  65.3 3.1 fusion
  68.4 43.5 %all-gather.12.cloned.1.call-done = bf16[2048,512]{1,0:T(8,128)(2,1)} async-done(((bf16[256,512]{1,0:T(8,128)(2,1)}), bf16[2048,512]{1,0:T(8,128)(2,1)}) %all-gather.12.cloned.1.call-update) | async-done | bytes 2097168 | tf_op jit(solution)/shard_map/all_gather | solution.py:60
  111.9 6.9 %fusion.21 = f32[1024,512]{1,0:T(8,128)} fusion(bf16[2048,512]{1,0:T(8,128)(2,1)} %all-gather.12.cloned.1.call-done, bf16[1024,2048]{1,0:T(8,128)(2,1)} %param.13, f32[2048]{0:T(1024)S(1)} %convert_element_type.48, f32[1024]{0:T(1024)S(1)} %add_rsqrt_fusion.2), kind=kOutput, calls=%fused_computation.30 | convolution fusion | flops 2160066560 | bytes 8400896 | tf_op jit(solution)/shard_map/dot_general | solution.py:63
  118.8 2.6 reshape.58
  121.4 1.2 reduce_sum.37
  122.6 14.4 %multiply_reduce_fusion = f32[1024,2]{1,0:T(8,128)S(1)} fusion(f32[1024,2,256]{2,1,0:T(2,128)S(1)} %reshape.58, f32[1024,2]{1,0:T(8,128)S(1)} %broadcast_multiply_fusion), kind=kLoop, calls=%fused_computation.33 | loop fusion | flops 1570816 | bytes 2113536 | tf_op jit(solution)/shard_map/reduce_sum | solution.py:19
  137.1 0.1 add_rsqrt_fusion
  137.2 1.2 mul.113
  138.4 0.2 copy.33
  138.6 0.0 copy-start
  138.6 1.2 sub.17
  139.9 0.2 copy.32
  140.0 0.4 copy-done
  140.4 0.0 copy-start.1
  140.4 0.8 add_convert_fusion.2
  141.3 0.3 reshape.59
  141.6 0.0 copy-done.1
  141.6 0.5 bitcast_add_fusion
  142.1 2.3 copy.27
  144.4 1.8 copy.34
  146.2 15.5 %all-gather.10.cloned.1.call-done = bf16[2048,512]{1,0:T(8,128)(2,1)} async-done(((bf16[256,512]{1,0:T(8,128)(2,1)}), bf16[2048,512]{1,0:T(8,128)(2,1)}) %all-gather.10.cloned.1.call-update) | async-done | bytes 2097168 | tf_op jit(solution)/shard_map/all_gather | solution.py:59
  161.7 5.7 %fusion.14 = bf16[1024,512]{1,0:T(8,128)(2,1)S(1)} fusion(f32[1024,512]{1,0:T(8,128)S(1)} %bitcast.40, bf16[2048,512]{1,0:T(8,128)(2,1)} %all-gather.10.cloned.1.call-done, bf16[1024,2048]{1,0:T(8,128)(2,1)} %param.13, f32[2048]{0:T(1024)S(1)} %convert_element_type.48, f32[1024]{0:T(1024)S(1)} %add_rsqrt_fusion.2), kind=kOutput, calls=%fused_computation.23 | convolution fusion | flops 2161115136 | bytes 9449472 | tf_op jit(solution)/shard_map/dot_general | solution.py:62
  167.4 0.5 copy.28
  168.0 4.6 all_to_all.38
  172.5 2.8 all-gather.16.cloned.1.call-done
  175.3 6.6 %add_convert_fusion.1 = bf16[512,2048]{1,0:T(8,128)(2,1)} fusion(bf16[512,1024]{0,1:T(8,128)(2,1)S(1)} %bitcast.37, bf16[1024,2048]{1,0:T(8,128)(2,1)} %all-gather.16.cloned.1.call-done, bf16[1024,2048]{1,0:T(8,128)(2,1)} %param.13, s32[]{:T(128)S(6)} %select_n.16), kind=kOutput, calls=%fused_computation.12 | convolution fusion | flops 2150629376 | bytes 9437188 | tf_op jit(solution)/shard_map/dot_general | solution.py:73
  181.9 0.0 copy-start.2
  181.9 0.0 all-gather.18.cloned.1.call-update
  181.9 0.0 all-gather.20.cloned.1.call-start
  182.0 0.7 all-gather.20.cloned.1.call-update
  182.7 0.0 all-gather.22.cloned.1.call-start
  182.7 0.7 all-gather.22.cloned.1.call-update
  183.4 0.0 all-gather.26.cloned.1.call-start
  183.5 88.1 %all-gather.24.cloned.1.call-done = bf16[1408,2048]{1,0:T(8,128)(2,1)} async-done(((bf16[1408,256]{1,0:T(8,128)(2,1)}), bf16[1408,2048]{1,0:T(8,128)(2,1)}) %all-gather.24.cloned.1.call-update) | async-done | bytes 5767184 | tf_op jit(solution)/shard_map/all_gather | solution.py:84
  271.6 0.0 all-gather.26.cloned.1.call-update
  271.6 0.0 copy-done.2
  271.6 13.2 %all-gather.18.cloned.1.call-done = bf16[1024,2048]{1,0:T(8,128)(2,1)} async-done(((bf16[512,2048]{1,0:T(8,128)(2,1)}), bf16[1024,2048]{1,0:T(8,128)(2,1)}) %all-gather.18.cloned.1.call-update) | async-done | bytes 4194320 | tf_op jit(solution)/shard_map/all_gather | solution.py:75
  284.8 3.1 fusion.3
  287.9 92.6 %all-gather.20.cloned.1.call-done = bf16[2048,1408]{1,0:T(8,128)(2,1)} async-done(((bf16[256,1408]{1,0:T(8,128)(2,1)}), bf16[2048,1408]{1,0:T(8,128)(2,1)}) %all-gather.20.cloned.1.call-update) | async-done | bytes 5767184 | tf_op jit(solution)/shard_map/all_gather | solution.py:78
  380.5 11.9 %fusion.23 = f32[1024,1408]{1,0:T(8,128)} fusion(bf16[2048,1408]{1,0:T(8,128)(2,1)} %all-gather.20.cloned.1.call-done, bf16[1024,2048]{1,0:T(8,128)(2,1)} %all-gather.18.cloned.1.call-done, f32[2048]{0:T(1024)S(1)} %convert_element_type.57, f32[1024]{0:T(1024)S(1)} %add_rsqrt_fusion.1), kind=kOutput, calls=%fused_computation.34 | convolution fusion | flops 5913968640 | bytes 15740928 | tf_op jit(solution)/shard_map/dot_general | solution.py:81
  392.4 80.8 %all-gather.22.cloned.1.call-done = bf16[2048,1408]{1,0:T(8,128)(2,1)} async-done(((bf16[256,1408]{1,0:T(8,128)(2,1)}), bf16[2048,1408]{1,0:T(8,128)(2,1)}) %all-gather.22.cloned.1.call-update) | async-done | bytes 5767184 | tf_op jit(solution)/shard_map/all_gather | solution.py:79
  473.2 12.5 %multiply_convert_fusion = bf16[1024,1408]{1,0:T(8,128)(2,1)} fusion(f32[1024,1408]{1,0:T(8,128)} %fusion.23, bf16[2048,1408]{1,0:T(8,128)(2,1)} %all-gather.22.cloned.1.call-done, bf16[1024,2048]{1,0:T(8,128)(2,1)} %all-gather.18.cloned.1.call-done, f32[2048]{0:T(1024)S(1)} %convert_element_type.57, f32[1024]{0:T(1024)S(1)} %add_rsqrt_fusion.1), kind=kOutput, calls=%fused_computation.10 | convolution fusion | flops 5922619392 | bytes 18624512 | tf_op jit(solution)/shard_map/dot_general | solution.py:82
  485.7 3.4 copy.29
  489.2 9.1 %all_to_all.39 = bf16[2,512,1408]{1,2,0:T(8,128)(2,1)} all-to-all(bf16[2,512,1408]{1,2,0:T(8,128)(2,1)S(1)} %copy.29), channel_id=1, replica_groups=mesh['rep'=2,'fs'=8,'tp'=2] {'tp'}, dimensions={0} | all-to-all | bytes 5767168 | tf_op jit(solution)/shard_map/all_to_all | solution.py:86
  498.3 0.5 all-gather.26.cloned.1.call-done
  498.8 11.1 %add_convert_fusion = bf16[512,2048]{1,0:T(8,128)(2,1)} fusion(bf16[512,2816]{0,1:T(8,128)(2,1)} %bitcast.38, bf16[2816,2048]{1,0:T(8,128)(2,1)} %all-gather.26.cloned.1.call-done, bf16[1024,2048]{1,0:T(8,128)(2,1)} %all-gather.18.cloned.1.call-done, s32[]{:T(128)S(6)} %select_n.16), kind=kOutput, calls=%fused_computation.11 | convolution fusion | flops 5908725760 | bytes 18612228 | tf_op jit(solution)/shard_map/dot_general | solution.py:88
  (5 shorter events, 0.1 us)
Async XLA Ops:
  6.5 55.9 %all-gather.14.cloned.1.call-start = ((), (), s32[]{:S(2)}) async-start(), calls=%async_computation.4 | async-start | bytes 2359296 | tf_op jit(solution)/shard_map/all_gather | solution.py:68
  7.3 104.7 %all-gather.12.cloned.1.call-start = ((), (), s32[]{:S(2)}) async-start(), calls=%async_computation.3 | async-start | bytes 2359296 | tf_op jit(solution)/shard_map/all_gather | solution.py:60
  8.0 153.7 %all-gather.10.cloned.1.call-start = ((), (), s32[]{:S(2)}) async-start(), calls=%async_computation.2 | async-start | bytes 2359296 | tf_op jit(solution)/shard_map/all_gather | solution.py:59
  8.7 166.6 %all-gather.16.cloned.1.call-start = ((), (), s32[]{:S(2)}) async-start(), calls=%async_computation.5 | async-start | bytes 6291456 | tf_op jit(solution)/shard_map/all_gather | solution.py:69
  62.5 209.1 %all-gather.24.cloned.1.call-start = ((), (), s32[]{:S(2)}) async-start(), calls=%async_computation.9 | async-start | bytes 6488064 | tf_op jit(solution)/shard_map/all_gather | solution.py:84
  63.1 221.8 %all-gather.18.cloned.1.call-start = ((), (), s32[]{:S(2)}) async-start(), calls=%async_computation.6 | async-start | bytes 6291456 | tf_op jit(solution)/shard_map/all_gather | solution.py:75
  138.6 1.8 copy-start
  140.4 1.1 copy-start.1
  181.9 89.7 %copy-start.2 = (bf16[2048]{0:T(1024)(128)(2,1)S(1)}, bf16[2048]{0:T(1024)(128)(2,1)}, u32[]{:S(2)}) copy-start(bf16[2048]{0:T(1024)(128)(2,1)} %param.22) | copy-start | bytes 12292
  181.9 198.6 %all-gather.20.cloned.1.call-start = ((), (), s32[]{:S(2)}) async-start(), calls=%async_computation.7 | async-start | bytes 6488064 | tf_op jit(solution)/shard_map/all_gather | solution.py:78
  182.7 290.6 %all-gather.22.cloned.1.call-start = ((), (), s32[]{:S(2)}) async-start(), calls=%async_computation.8 | async-start | bytes 6488064 | tf_op jit(solution)/shard_map/all_gather | solution.py:79
  183.4 315.3 %all-gather.26.cloned.1.call-start = ((), (), s32[]{:S(2)}) async-start(), calls=%async_computation.10 | async-start | bytes 17301504 | tf_op jit(solution)/shard_map/all_gather | solution.py:87
Sparse Core Ops, SparseCore 0:
  9.4 53.0 all-gather.13
  64.6 47.2 all-gather.11
  114.0 47.6 all-gather.9
  163.1 12.1 all-gather.15
  177.2 94.2 all-gather.23
  273.0 11.8 all-gather.17
  287.0 93.4 all-gather.19
  382.7 90.4 all-gather.21
  474.8 23.8 all-gather.25
where the time goes:
time: 517 us; the launch traced here: 516 us
  waiting for transfers between devices  395 us (76%)
  matrix products  55.2 us (11%)
  other arithmetic  24.9 us (5%)
  local copies, waits for them, and re-layouts  14.2 us (3%)
  blocking collectives  13.7 us (3%)
  between operations  13.4 us (3%)
    all_gather x1, waiting for transfers between devices, on_device(): lax.all_gather(w_gate, 'fs', axis=0, tiled=True)  92.6 us
    all_gather x1, waiting for transfers between devices, on_device(): down_cols = lax.all_gather(w_down, 'fs', axis=1, tiled=True)  88.1 us
    all_gather x1, waiting for transfers between devices, on_device(): lax.all_gather(w_up, 'fs', axis=0, tiled=True)  80.8 us
    all_gather x1, waiting for transfers between devices, on_device(): out_columns = lax.all_gather(w_mix_out, 'fs', axis=1, tiled=True)  53.7 us
    all_gather x1, waiting for transfers between devices, on_device(): lax.all_gather(w_value, 'fs', axis=0, tiled=True)  43.5 us
    all_gather x1, waiting for transfers between devices, on_device(): lax.all_gather(w_unit, 'fs', axis=0, tiled=True)  15.5 us
    reduce_sum x1, other arithmetic, spatial_unit(): spread = jnp.mean(jnp.square(active - center), axis=-1, keepdims=True)  14.4 us
    all_gather x1, waiting for transfers between devices, on_device(): h_mid = lax.all_gather(own_mid, 'tp', axis=0, tiled=True)  13.2 us
  transfers between devices with their start and end apart: 9, of which 9 were waited for; matrix products, arithmetic and copies ran while one was open for 16% of the time, Pallas kernels for 0%

commit v1 on v0

--- a/solution.py
+++ b/solution.py
@@ -81,7 +81,12 @@
     gate = jnp.dot(normed_mid, gate_whole, preferred_element_type=jnp.float32)
     up = jnp.dot(normed_mid, up_whole, preferred_element_type=jnp.float32)
     hidden = (jax.nn.silu(gate) * up).astype(jnp.bfloat16)
-    down_cols = lax.all_gather(w_down, "fs", axis=1, tiled=True)
+    ring = [w_down]
+    for hop in range(7):
+        ring.append(lax.ppermute(ring[-1], "fs", [(dev, (dev + 1) % 8) for dev in range(8)]))
+    down_cols = jnp.roll(
+        jnp.concatenate(ring[::-1], axis=1), (lax.axis_index("fs") + 1) * ring[0].shape[1], axis=1
+    )
     residual_rows = lax.dynamic_slice_in_dim(h_mid, row_start, half, 0).astype(jnp.float32)
     hidden_rows = lax.all_to_all(hidden, "tp", split_axis=0, concat_axis=1, tiled=True)
     down_full = lax.all_gather(down_cols, "tp", axis=0, tiled=True)

time: 517 us -> 498 us (0.963)
  waiting for transfers between devices: 395 us -> 360 us
  local copies, waits for them, and re-layouts: 14.2 us -> 26.6 us
    ppermute x0 -> x7, waiting for transfers between devices: none -> 207 us  [on_device(): lax.ppermute(ring[-1], 'fs', [(dev, (dev + 1) % 8) for dev in range(8)])]
    all_gather x1, waiting for transfers between devices: 92.6 us -> 0.02 us  [on_device(): lax.all_gather(w_gate, 'fs', axis=0, tiled=True)]
    all_gather x1 -> x0, waiting for transfers between devices: 88.1 us -> none  [on_device(): down_cols = lax.all_gather(w_down, 'fs', axis=1, tiled=True)]
    all_gather x1, waiting for transfers between devices: 80.8 us -> 33.9 us  [on_device(): lax.all_gather(w_up, 'fs', axis=0, tiled=True)]
    all_gather x1, waiting for transfers between devices: 13.2 us -> 0.01 us  [on_device(): h_mid = lax.all_gather(own_mid, 'tp', axis=0, tiled=True)]
    unnamed x9 -> x34, local copies, waits for them, and re-layouts: 2.53 us -> 11.9 us
  transfers between devices with their start and end apart: 9 -> 15, of which waited for: 9 -> 13; matrix products, arithmetic and copies ran while one was open for 16% -> 17% of each run, Pallas kernels for 0% -> 0%
where the time goes in v1:
time: 498 us; the launch traced here: 497 us
  waiting for transfers between devices  360 us (72%)
  matrix products  55.3 us (11%)
  local copies, waits for them, and re-layouts  26.6 us (5%)
  other arithmetic  24.9 us (5%)
  between operations  13.8 us (3%)
  blocking collectives  13.7 us (3%)
    ppermute x7, waiting for transfers between devices, on_device(): lax.ppermute(ring[-1], 'fs', [(dev, (dev + 1) % 8) for dev in range(8)])  207 us
    all_gather x1, waiting for transfers between devices, on_device(): out_columns = lax.all_gather(w_mix_out, 'fs', axis=1, tiled=True)  53.7 us
    all_gather x1, waiting for transfers between devices, on_device(): lax.all_gather(w_value, 'fs', axis=0, tiled=True)  44.1 us
    all_gather x1, waiting for transfers between devices, on_device(): lax.all_gather(w_up, 'fs', axis=0, tiled=True)  33.9 us
    all_gather x1, waiting for transfers between devices, on_device(): lax.all_gather(w_unit, 'fs', axis=0, tiled=True)  15.5 us
    reduce_sum x1, other arithmetic, spatial_unit(): spread = jnp.mean(jnp.square(active - center), axis=-1, keepdims=True)  14.4 us
    dot_general x1, matrix products, on_device(): up = jnp.dot(normed_mid, up_whole, preferred_element_type=jnp.float32)  12.4 us
    dot_general x1, matrix products, on_device(): gate = jnp.dot(normed_mid, gate_whole, preferred_element_type=jnp.float32)  11.9 us
  transfers between devices with their start and end apart: 15, of which 13 were waited for; matrix products, arithmetic and copies ran while one was open for 17% of the time, Pallas kernels for 0%

profile of v1, /device:TPU:0, one launch (start us, length us, event | category | flops | bytes accessed | tf_op | source)
XLA Modules:
  0.0 496.8 jit_solution(18067115918367499886)
XLA Ops:
  6.5 0.7 all-gather.13.cloned.1.call-update
  7.3 0.7 all-gather.11.cloned.1.call-update
  8.1 0.7 all-gather.9.cloned.1.call-update
  8.8 53.7 %all-gather.13.cloned.1.call-done = bf16[512,2048]{1,0:T(8,128)(2,1)} async-done(((bf16[512,256]{1,0:T(8,128)(2,1)}), bf16[512,2048]{1,0:T(8,128)(2,1)}) %all-gather.13.cloned.1.call-update) | async-done | bytes 2097168 | tf_op jit(solution)/shard_map/all_gather | solution.py:68
  62.6 0.7 convert_element_type.48
  63.2 0.7 convert_bitcast_fusion
  63.9 0.8 dynamic-slice_convert_fusion
  64.7 3.1 fusion
  67.8 44.1 %all-gather.11.cloned.1.call-done = bf16[2048,512]{1,0:T(8,128)(2,1)} async-done(((bf16[256,512]{1,0:T(8,128)(2,1)}), bf16[2048,512]{1,0:T(8,128)(2,1)}) %all-gather.11.cloned.1.call-update) | async-done | bytes 2097168 | tf_op jit(solution)/shard_map/all_gather | solution.py:60
  111.9 6.9 %fusion.21 = f32[1024,512]{1,0:T(8,128)} fusion(bf16[2048,512]{1,0:T(8,128)(2,1)} %all-gather.11.cloned.1.call-done, bf16[1024,2048]{1,0:T(8,128)(2,1)} %param.13, f32[2048]{0:T(1024)S(1)} %convert_element_type.48, f32[1024]{0:T(1024)S(1)} %add_rsqrt_fusion.2), kind=kOutput, calls=%fused_computation.30 | convolution fusion | flops 2160066560 | bytes 8400896 | tf_op jit(solution)/shard_map/dot_general | solution.py:63
  118.8 2.6 reshape.58
  121.4 1.2 reduce_sum.37
  122.6 14.4 %multiply_reduce_fusion = f32[1024,2]{1,0:T(8,128)S(1)} fusion(f32[1024,2,256]{2,1,0:T(2,128)S(1)} %reshape.58, f32[1024,2]{1,0:T(8,128)S(1)} %broadcast_multiply_fusion), kind=kLoop, calls=%fused_computation.33 | loop fusion | flops 1570816 | bytes 2113536 | tf_op jit(solution)/shard_map/reduce_sum | solution.py:19
  137.2 1.2 mul.116
  138.4 0.2 copy.33
  138.6 1.2 sub.21
  139.9 0.2 copy.32
  140.0 0.4 copy-done
  140.4 0.8 add_convert_fusion.2
  141.3 0.3 reshape.59
  141.6 0.5 bitcast_add_fusion
  142.1 2.3 copy.27
  144.4 1.8 copy.34
  146.2 15.5 %all-gather.9.cloned.1.call-done = bf16[2048,512]{1,0:T(8,128)(2,1)} async-done(((bf16[256,512]{1,0:T(8,128)(2,1)}), bf16[2048,512]{1,0:T(8,128)(2,1)}) %all-gather.9.cloned.1.call-update) | async-done | bytes 2097168 | tf_op jit(solution)/shard_map/all_gather | solution.py:59
  161.7 5.7 %fusion.14 = bf16[1024,512]{1,0:T(8,128)(2,1)S(1)} fusion(f32[1024,512]{1,0:T(8,128)S(1)} %bitcast.40, bf16[2048,512]{1,0:T(8,128)(2,1)} %all-gather.9.cloned.1.call-done, bf16[1024,2048]{1,0:T(8,128)(2,1)} %param.13, f32[2048]{0:T(1024)S(1)} %convert_element_type.48, f32[1024]{0:T(1024)S(1)} %add_rsqrt_fusion.2), kind=kOutput, calls=%fused_computation.23 | convolution fusion | flops 2161115136 | bytes 9449472 | tf_op jit(solution)/shard_map/dot_general | solution.py:62
  167.4 0.5 copy.28
  168.0 4.6 all_to_all.38
  172.5 2.8 all-gather.15.cloned.1.call-done
  175.3 6.6 %add_convert_fusion.1 = bf16[512,2048]{1,0:T(8,128)(2,1)} fusion(bf16[512,1024]{0,1:T(8,128)(2,1)S(1)} %bitcast.37, bf16[1024,2048]{1,0:T(8,128)(2,1)} %all-gather.15.cloned.1.call-done, bf16[1024,2048]{1,0:T(8,128)(2,1)} %param.13, s32[]{:T(128)S(6)} %select_n.29), kind=kOutput, calls=%fused_computation.12 | convolution fusion | flops 2150629376 | bytes 9437188 | tf_op jit(solution)/shard_map/dot_general | solution.py:73
  182.0 0.5 all-gather.19.cloned.1.call-update
  182.6 0.7 all-gather.21.cloned.1.call-update
  183.4 1.8 collective-permute-start
  185.2 19.4 %collective-permute-done = bf16[1408,256]{1,0:T(8,128)(2,1)S(1)} collective-permute-done((bf16[1408,256]{1,0:T(8,128)(2,1)S(1)}, bf16[1408,256]{1,0:T(8,128)(2,1)S(1)}, u32[]{:S(2)}, u32[]{:S(2)}) %collective-permute-start) | collective-permute-done | bytes 720928 | tf_op jit(solution)/shard_map/ppermute | solution.py:86
  204.5 32.3 %collective-permute-done.1 = bf16[1408,256]{1,0:T(8,128)(2,1)S(1)} collective-permute-done((bf16[1408,256]{1,0:T(8,128)(2,1)S(1)}, bf16[1408,256]{1,0:T(8,128)(2,1)S(1)}, u32[]{:S(2)}, u32[]{:S(2)}) %collective-permute-start.1) | collective-permute-done | bytes 720928 | tf_op jit(solution)/shard_map/ppermute | solution.py:86
  236.9 26.7 %collective-permute-done.2 = bf16[1408,256]{1,0:T(8,128)(2,1)S(1)} collective-permute-done((bf16[1408,256]{1,0:T(8,128)(2,1)S(1)}, bf16[1408,256]{1,0:T(8,128)(2,1)S(1)}, u32[]{:S(2)}, u32[]{:S(2)}) %collective-permute-start.2) | collective-permute-done | bytes 720928 | tf_op jit(solution)/shard_map/ppermute | solution.py:86
  263.6 36.3 %collective-permute-done.3 = bf16[1408,256]{1,0:T(8,128)(2,1)S(1)} collective-permute-done((bf16[1408,256]{1,0:T(8,128)(2,1)S(1)}, bf16[1408,256]{1,0:T(8,128)(2,1)S(1)}, u32[]{:S(2)}, u32[]{:S(2)}) %collective-permute-start.3) | collective-permute-done | bytes 720928 | tf_op jit(solution)/shard_map/ppermute | solution.py:86
  299.9 0.9 copy-done.2
  300.8 36.1 %collective-permute-done.4 = bf16[1408,256]{1,0:T(8,128)(2,1)S(1)} collective-permute-done((bf16[1408,256]{1,0:T(8,128)(2,1)S(1)}, bf16[1408,256]{1,0:T(8,128)(2,1)S(1)}, u32[]{:S(2)}, u32[]{:S(2)}) %collective-permute-start.4) | collective-permute-done | bytes 720928 | tf_op jit(solution)/shard_map/ppermute | solution.py:86
  336.9 0.9 copy-done.4
  337.7 19.5 %collective-permute-done.5 = bf16[1408,256]{1,0:T(8,128)(2,1)} collective-permute-done((bf16[1408,256]{1,0:T(8,128)(2,1)S(1)}, bf16[1408,256]{1,0:T(8,128)(2,1)}, u32[]{:S(2)}, u32[]{:S(2)}) %collective-permute-start.5) | collective-permute-done | bytes 720928 | tf_op jit(solution)/shard_map/ppermute | solution.py:86
  357.3 36.3 %collective-permute-done.6 = bf16[1408,256]{1,0:T(8,128)(2,1)} collective-permute-done((bf16[1408,256]{1,0:T(8,128)(2,1)}, bf16[1408,256]{1,0:T(8,128)(2,1)}, u32[]{:S(2)}, u32[]{:S(2)}) %collective-permute-start.6) | collective-permute-done | bytes 720928 | tf_op jit(solution)/shard_map/ppermute | solution.py:86
  393.6 1.2 constant_dynamic-update-slice_fusion.15
  394.8 1.2 constant_dynamic-update-slice_fusion.14
  396.0 1.2 constant_dynamic-update-slice_fusion.13
  397.4 0.1 constant_dynamic-update-slice_fusion.10
  397.5 0.1 constant_dynamic-update-slice_fusion.9
  397.6 0.1 constant_dynamic-update-slice_fusion.8
  397.7 1.2 constant_dynamic-update-slice_fusion.7
  398.9 1.2 constant_dynamic-update-slice_fusion.6
  400.3 0.1 constant_dynamic-update-slice_fusion.4
  400.4 0.1 constant_dynamic-update-slice_fusion.3
  400.5 0.1 constant_dynamic-update-slice_fusion.2
  400.6 0.1 constant_dynamic-update-slice_fusion.1
  400.7 0.1 constant_dynamic-update-slice_fusion
  400.8 3.0 constant_dynamic-slice_fusion
  403.8 0.7 copy-done.7
  404.4 3.1 fusion.3
  407.6 11.9 %fusion.23 = f32[1024,1408]{1,0:T(8,128)} fusion(bf16[2048,1408]{1,0:T(8,128)(2,1)} %all-gather.19.cloned.1.call-done, bf16[1024,2048]{1,0:T(8,128)(2,1)} %all-gather.17.cloned.1.call-done, f32[2048]{0:T(1024)S(1)} %convert_element_type.57, f32[1024]{0:T(1024)S(1)} %add_rsqrt_fusion.1), kind=kOutput, calls=%fused_computation.34 | convolution fusion | flops 5913968640 | bytes 15740928 | tf_op jit(solution)/shard_map/dot_general | solution.py:81
  419.5 33.9 %all-gather.21.cloned.1.call-done = bf16[2048,1408]{1,0:T(8,128)(2,1)} async-done(((bf16[256,1408]{1,0:T(8,128)(2,1)}), bf16[2048,1408]{1,0:T(8,128)(2,1)}) %all-gather.21.cloned.1.call-update) | async-done | bytes 5767184 | tf_op jit(solution)/shard_map/all_gather | solution.py:79
  453.4 12.4 %multiply_convert_fusion = bf16[1024,1408]{1,0:T(8,128)(2,1)} fusion(f32[1024,1408]{1,0:T(8,128)} %fusion.23, bf16[2048,1408]{1,0:T(8,128)(2,1)} %all-gather.21.cloned.1.call-done, bf16[1024,2048]{1,0:T(8,128)(2,1)} %all-gather.17.cloned.1.call-done, f32[2048]{0:T(1024)S(1)} %convert_element_type.57, f32[1024]{0:T(1024)S(1)} %add_rsqrt_fusion.1), kind=kOutput, calls=%fused_computation.10 | convolution fusion | flops 5922619392 | bytes 18624512 | tf_op jit(solution)/shard_map/dot_general | solution.py:82
  465.8 3.4 copy.29
  469.3 9.1 %all_to_all.39 = bf16[2,512,1408]{1,2,0:T(8,128)(2,1)} all-to-all(bf16[2,512,1408]{1,2,0:T(8,128)(2,1)S(1)} %copy.29), channel_id=1, replica_groups=mesh['rep'=2,'fs'=8,'tp'=2] {'tp'}, dimensions={0} | all-to-all | bytes 5767168 | tf_op jit(solution)/shard_map/all_to_all | solution.py:91
  478.4 0.5 all-gather.23.cloned.1.call-done
  478.9 11.1 %add_convert_fusion = bf16[512,2048]{1,0:T(8,128)(2,1)} fusion(bf16[512,2816]{0,1:T(8,128)(2,1)} %bitcast.38, bf16[2816,2048]{1,0:T(8,128)(2,1)} %all-gather.23.cloned.1.call-done, bf16[1024,2048]{1,0:T(8,128)(2,1)} %all-gather.17.cloned.1.call-done, s32[]{:T(128)S(6)} %select_n.29), kind=kOutput, calls=%fused_computation.11 | convolution fusion | flops 5908725760 | bytes 18612228 | tf_op jit(solution)/shard_map/dot_general | solution.py:93
  (40 shorter events, 0.8 us)
Async XLA Ops:
  6.5 55.9 %all-gather.13.cloned.1.call-start = ((), (), s32[]{:S(2)}) async-start(), calls=%async_computation.4 | async-start | bytes 2359296 | tf_op jit(solution)/shard_map/all_gather | solution.py:68
  7.3 104.7 %all-gather.11.cloned.1.call-start = ((), (), s32[]{:S(2)}) async-start(), calls=%async_computation.3 | async-start | bytes 2359296 | tf_op jit(solution)/shard_map/all_gather | solution.py:60
  8.0 153.7 %all-gather.9.cloned.1.call-start = ((), (), s32[]{:S(2)}) async-start(), calls=%async_computation.2 | async-start | bytes 2359296 | tf_op jit(solution)/shard_map/all_gather | solution.py:59
  8.7 166.6 %all-gather.15.cloned.1.call-start = ((), (), s32[]{:S(2)}) async-start(), calls=%async_computation.5 | async-start | bytes 6291456 | tf_op jit(solution)/shard_map/all_gather | solution.py:69
  62.5 341.9 %all-gather.17.cloned.1.call-start = ((), (), s32[]{:S(2)}) async-start(), calls=%async_computation.6 | async-start | bytes 6291456 | tf_op jit(solution)/shard_map/all_gather | solution.py:75
  138.6 1.8 copy-start
  140.4 1.1 copy-start.6
  175.3 8.0 %copy-start.1 = (bf16[1408,256]{1,0:T(8,128)(2,1)S(1)}, bf16[1408,256]{1,0:T(8,128)(2,1)}, u32[]{:S(2)}) copy-start(bf16[1408,256]{1,0:T(8,128)(2,1)} %param.25) | copy-start | bytes 2162692
  182.0 225.6 %all-gather.19.cloned.1.call-start = ((), (), s32[]{:S(2)}) async-start(), calls=%async_computation.7 | async-start | bytes 6488064 | tf_op jit(solution)/shard_map/all_gather | solution.py:78
  182.6 270.8 %all-gather.21.cloned.1.call-start = ((), (), s32[]{:S(2)}) async-start(), calls=%async_computation.8 | async-start | bytes 6488064 | tf_op jit(solution)/shard_map/all_gather | solution.py:79
  183.3 295.6 %all-gather.23.cloned.1.call-start = ((), (), s32[]{:S(2)}) async-start(), calls=%async_computation.9 | async-start | bytes 17301504 | tf_op jit(solution)/shard_map/all_gather | solution.py:92
  183.4 21.2 %collective-permute-start = (bf16[1408,256]{1,0:T(8,128)(2,1)S(1)}, bf16[1408,256]{1,0:T(8,128)(2,1)S(1)}, u32[]{:S(2)}, u32[]{:S(2)}) collective-permute-start(bf16[1408,256]{1,0:T(8,128)(2,1)S(1)} %copy-done.1), channel_id=1, source_target_pairs={{0,2},{2,4},{4,6},{6,8},{8,10},{10,12},{12,14},{14,0},{1,3},{3,5},... | collective-permute-start | bytes 2162696 | tf_op jit(solution)/shard_map/ppermute | solution.py:86
  204.5 32.3 %collective-permute-start.1 = (bf16[1408,256]{1,0:T(8,128)(2,1)S(1)}, bf16[1408,256]{1,0:T(8,128)(2,1)S(1)}, u32[]{:S(2)}, u32[]{:S(2)}) collective-permute-start(bf16[1408,256]{1,0:T(8,128)(2,1)S(1)} %collective-permute-done), channel_id=1, source_target_pairs={{0,2},{2,4},{4,6},{6,8},{8,10},{10,12},{12,14},{14,0},{1,3},{3,5},... | collective-permute-start | bytes 2162696 | tf_op jit(solution)/shard_map/ppermute | solution.py:86
  236.8 26.7 %collective-permute-start.2 = (bf16[1408,256]{1,0:T(8,128)(2,1)S(1)}, bf16[1408,256]{1,0:T(8,128)(2,1)S(1)}, u32[]{:S(2)}, u32[]{:S(2)}) collective-permute-start(bf16[1408,256]{1,0:T(8,128)(2,1)S(1)} %collective-permute-done.1), channel_id=1, source_target_pairs={{0,2},{2,4},{4,6},{6,8},{8,10},{10,12},{12,14},{14,0},{1,3},{3,5},... | collective-permute-start | bytes 2162696 | tf_op jit(solution)/shard_map/ppermute | solution.py:86
  263.6 36.3 %collective-permute-start.3 = (bf16[1408,256]{1,0:T(8,128)(2,1)S(1)}, bf16[1408,256]{1,0:T(8,128)(2,1)S(1)}, u32[]{:S(2)}, u32[]{:S(2)}) collective-permute-start(bf16[1408,256]{1,0:T(8,128)(2,1)S(1)} %collective-permute-done.2), channel_id=1, source_target_pairs={{0,2},{2,4},{4,6},{6,8},{8,10},{10,12},{12,14},{14,0},{1,3},{3,5},... | collective-permute-start | bytes 2162696 | tf_op jit(solution)/shard_map/ppermute | solution.py:86
  299.9 0.9 copy-start.2
  300.8 36.1 %collective-permute-start.4 = (bf16[1408,256]{1,0:T(8,128)(2,1)S(1)}, bf16[1408,256]{1,0:T(8,128)(2,1)S(1)}, u32[]{:S(2)}, u32[]{:S(2)}) collective-permute-start(bf16[1408,256]{1,0:T(8,128)(2,1)S(1)} %collective-permute-done.3), channel_id=1, source_target_pairs={{0,2},{2,4},{4,6},{6,8},{8,10},{10,12},{12,14},{14,0},{1,3},{3,5},... | collective-permute-start | bytes 2162696 | tf_op jit(solution)/shard_map/ppermute | solution.py:86
  336.9 0.9 copy-start.4
  337.7 19.5 %collective-permute-start.5 = (bf16[1408,256]{1,0:T(8,128)(2,1)S(1)}, bf16[1408,256]{1,0:T(8,128)(2,1)}, u32[]{:S(2)}, u32[]{:S(2)}) collective-permute-start(bf16[1408,256]{1,0:T(8,128)(2,1)S(1)} %collective-permute-done.4), channel_id=1, source_target_pairs={{0,2},{2,4},{4,6},{6,8},{8,10},{10,12},{12,14},{14,0},{1,3},{3,5},... | collective-permute-start | bytes 2162696 | tf_op jit(solution)/shard_map/ppermute | solution.py:86
  357.2 36.3 %collective-permute-start.6 = (bf16[1408,256]{1,0:T(8,128)(2,1)}, bf16[1408,256]{1,0:T(8,128)(2,1)}, u32[]{:S(2)}, u32[]{:S(2)}) collective-permute-start(bf16[1408,256]{1,0:T(8,128)(2,1)} %collective-permute-done.5), channel_id=1, source_target_pairs={{0,2},{2,4},{4,6},{6,8},{8,10},{10,12},{12,14},{14,0},{1,3},{3,5},... | collective-permute-start | bytes 2162696 | tf_op jit(solution)/shard_map/ppermute | solution.py:86
  357.3 40.0 %copy-start.3 = (bf16[1408,256]{1,0:T(8,128)(2,1)S(1)}, bf16[1408,256]{1,0:T(8,128)(2,1)}, u32[]{:S(2)}) copy-start(bf16[1408,256]{1,0:T(8,128)(2,1)} %copy-done.2) | copy-start | bytes 2162692
  397.3 2.8 copy-start.5
  403.7 0.7 copy-start.7
Sparse Core Ops, SparseCore 0:
  9.4 53.0 all-gather.12
  64.6 47.2 all-gather.10
  114.0 47.6 all-gather.8
  163.1 12.1 all-gather.14
  182.1 14.8 all-gather.16
  199.0 134.8 all-gather.18
  336.1 117.2 all-gather.20
  454.9 23.9 all-gather.22
